TPU v7x, 128 devices: a whole 4x4x4 slice. The times are simulated.
128 devices in a mesh: sp: 16 (over z, x), tp: 8 (over y, core).
Axes of the slice: x: 4, y: 4, z: 4, core: 2. Of those that a mesh axis runs over, the one named last changes fastest.
Arguments:
- query_narrow: bfloat16 [4096, 1024], P('sp', 'tp'), may hold values from -6 to 6
- key_narrow: bfloat16 [4096, 1024], P('sp', 'tp'), may hold values from -6 to 6
- value_narrow: bfloat16 [4096, 1024], P('sp', 'tp'), may hold values from -12 to 12
- query_broad: bfloat16 [4096, 1024], P('sp', 'tp'), may hold values from -6 to 6
- key_broad: bfloat16 [4096, 1024], P('sp', 'tp'), may hold values from -6 to 6
- value_broad: bfloat16 [4096, 1024], P('sp', 'tp'), may hold values from -12 to 12
- offset_narrow: bfloat16 [16, 4096], P('tp', 'sp'), as said below
- offset_broad: bfloat16 [8, 4096], P('tp', 'sp'), as said below
- residual: bfloat16 [4096, 2048], P(('sp', 'tp')), may hold values from -6 to 6
- out_narrow: bfloat16 [1024, 2048], P('tp'), may hold values from -0.25 to 0.25
- out_broad: bfloat16 [1024, 2048], P('tp'), may hold values from -0.25 to 0.25
- norm_gain: float32 [2048], replicated, may hold values from 0.1 to 1.9
- up_proj: bfloat16 [2048, 8192], P('sp', 'tp'), may hold values from -0.125 to 0.125
- down_proj: bfloat16 [8192, 2048], P('tp', 'sp'), may hold values from -0.0625 to 0.0625
Outputs:
- output: bfloat16 [4096, 2048], P(('sp', 'tp'))
Inputs may be any that keep to these rules, and one draw needn't show every extreme that they name: `offset_narrow`: additive score offsets of each head for each key position. `offset_broad`: additive score offsets of each head for each key position.
All inputs are finite; a program needn't handle non-finite values.
Results may differ from a plain program's by a relative error of at most 0.018.
Values may be sent and summed in bfloat16 or wider, within the bound.
A program may use at most 64 MiB of HBM per device.

v0:
```python
import math
import jax
import jax.numpy as jnp
from jax import lax
from jax.sharding import PartitionSpec as P

NARROW_SIZE = 64
BROAD_SIZE = 128


def turned_gather(arrays, axis, dims):
    turned = [jnp.moveaxis(a, dim, 0) for a, dim in zip(arrays, dims)]
    widths = [t[0].size for t in turned]
    both = jnp.concatenate([t.reshape(-1, w) for t, w in zip(turned, widths)], axis=1)
    whole = lax.all_gather(both, axis, axis=0, tiled=True)
    tiles = jnp.split(whole, [sum(widths[:k]) for k in range(1, len(widths))], axis=1)
    return tuple(
        (
            jnp.moveaxis(b.reshape(-1, *t.shape[1:]), 0, dim)
            for b, t, dim in zip(tiles, turned, dims)
        )
    )


def cut_along(value, dim, count):
    dims = value.shape
    tiles = value.reshape(*dims[:dim], count, dims[dim] // count, *dims[dim + 1 :])
    return jnp.moveaxis(tiles, dim, 0)


def summed_on_arrival(value, axis, dim):
    count = lax.axis_size(axis)
    tiles = lax.all_to_all(cut_along(value, dim, count), axis, 0, 0, tiled=True)
    return jnp.sum(tiles.astype(jnp.float32), axis=0)


def from_everyone(value, axis):
    copies = jnp.broadcast_to(value, (lax.axis_size(axis), *value.shape))
    return lax.all_to_all(copies, axis, split_axis=0, concat_axis=0, tiled=True)


def in_order(tiles, dim):
    dims = list(tiles.shape[1:])
    dims[dim] *= tiles.shape[0]
    return jnp.moveaxis(tiles, 0, dim).reshape(dims)


def collect(value, axis, dim):
    tiles = from_everyone(value, axis)
    return in_order(tiles, dim)


def on_gathered_pieces(value, axis, dim, work, out_dim):
    width = value.shape[dim]
    pieces = jnp.split(value, 2, axis=dim) if width % 2 == 0 else [value]
    leading = jnp.arange(lax.axis_size(axis)) * width
    tiles = [lax.all_gather(share, axis) for share in pieces]
    made = [jax.vmap(work)(b, leading + k * (width // len(pieces))) for k, b in enumerate(tiles)]
    return in_order(jnp.concatenate(made, axis=out_dim + 1), out_dim)


def stick_block(state, query, keys_block, values_block, offsets, query_pos, key_pos, head_size):
    keep_sum, running = state
    row_count = query.shape[0]
    total_heads = query.shape[1] // head_size
    key_count = keys_block.shape[0]
    q_heads = query.reshape(row_count, total_heads, head_size)
    k_heads = keys_block.reshape(key_count, total_heads, head_size)
    v_heads = values_block.reshape(key_count, total_heads, head_size)
    scores = jnp.einsum(
        "qhe,khe->hqk", q_heads, k_heads, preferred_element_type=jnp.float32
    ) * head_size ** (-0.5)
    scores = scores + offsets.astype(jnp.float32)[:, None, :]
    causal = (key_pos[None, :] < query_pos[:, None])[None]
    log_keep = jnp.where(causal, jax.nn.log_sigmoid(-scores), 0.0)
    keep_after = lax.cumsum(log_keep, axis=2, reverse=True) - log_keep
    weight = jnp.where(
        causal, jnp.exp(jax.nn.log_sigmoid(scores) + keep_after + keep_sum[:, :, None]), 0.0
    )
    weight = weight.astype(jnp.bfloat16)
    running = running + jnp.einsum(
        "hqk,khe->qhe", weight, v_heads, preferred_element_type=jnp.float32
    )
    return (keep_sum + jnp.sum(log_keep, axis=2), running)


def attend_block(states, pieces, query_pos, key_pos, queries):
    key_n, value_n, key_b, value_b, off_n, off_b = pieces
    state_narrow = stick_block(
        states[0], queries[0], key_n, value_n, off_n, query_pos, key_pos, NARROW_SIZE
    )
    state_broad = stick_block(
        states[1], queries[1], key_b, value_b, off_b, query_pos, key_pos, BROAD_SIZE
    )
    return (state_narrow, state_broad)


def local(
    query_narrow,
    key_narrow,
    value_narrow,
    query_broad,
    key_broad,
    value_broad,
    offset_narrow,
    offset_broad,
    residual,
    out_narrow,
    out_broad,
    norm_gain,
    up_proj,
    down_proj,
):
    tok_dev = query_narrow.shape[0]
    my_shard = lax.axis_index("sp")
    query_pos = my_shard * tok_dev + jnp.arange(tok_dev, dtype=jnp.int32)
    queries = (query_narrow, query_broad)

    def empty_state(total_heads, head_size):
        return (
            jnp.zeros((total_heads, tok_dev), jnp.float32),
            jnp.zeros((tok_dev, total_heads, head_size), jnp.float32),
        )

    states = (
        empty_state(offset_narrow.shape[0], NARROW_SIZE),
        empty_state(offset_broad.shape[0], BROAD_SIZE),
    )
    own_keys = (key_narrow, value_narrow, key_broad, value_broad, offset_narrow, offset_broad)
    whole_keys = turned_gather(
        (own_keys[0], own_keys[1], own_keys[2], own_keys[3], own_keys[4], own_keys[5]),
        "sp",
        (0, 0, 0, 0, 1, 1),
    )
    key_span = math.gcd(tok_dev, 512)
    block_count = (my_shard + 1) * (tok_dev // key_span)

    def sweep(turn_index, current):
        first_row = (block_count - 1 - turn_index) * key_span
        row_pieces = tuple(
            (lax.dynamic_slice_in_dim(array, first_row, key_span, 0) for array in whole_keys[:4])
        )
        col_pieces = tuple(
            (lax.dynamic_slice_in_dim(array, first_row, key_span, 1) for array in whole_keys[4:])
        )
        key_pos = first_row + jnp.arange(key_span, dtype=jnp.int32)
        return attend_block(current, row_pieces + col_pieces, query_pos, key_pos, queries)

    states = lax.fori_loop(0, block_count, sweep, states)
    mixed_narrow = states[0][1].reshape(tok_dev, -1).astype(jnp.bfloat16)
    mixed_broad = states[1][1].reshape(tok_dev, -1).astype(jnp.bfloat16)
    attended = summed_on_arrival(
        (
            jnp.dot(mixed_narrow, out_narrow, preferred_element_type=jnp.float32)
            + jnp.dot(mixed_broad, out_broad, preferred_element_type=jnp.float32)
        ).astype(jnp.bfloat16),
        "tp",
        0,
    )
    updated = residual.astype(jnp.float32) + attended
    scale = lax.rsqrt(jnp.mean(updated * updated, axis=-1, keepdims=True) + 1e-06)
    normed = (updated * scale * norm_gain).astype(jnp.bfloat16)
    gathered = collect(normed, "tp", 0)
    pre_act = jnp.dot(
        gathered,
        lax.all_gather(up_proj, "sp", axis=0, tiled=True),
        preferred_element_type=jnp.float32,
    )
    hidden = jnp.square(jax.nn.relu(pre_act)).astype(jnp.bfloat16)

    def project(shard_piece, row_start):
        return jnp.dot(hidden, shard_piece, preferred_element_type=jnp.float32)

    partial_sums = on_gathered_pieces(down_proj, "sp", 1, project, 1)
    channel = summed_on_arrival(partial_sums.astype(jnp.bfloat16), "tp", 0)
    return (updated + channel).astype(jnp.bfloat16)


def solution(mesh):
    return jax.shard_map(
        local,
        mesh=mesh,
        in_specs=(
            P("sp", "tp"),
            P("sp", "tp"),
            P("sp", "tp"),
            P("sp", "tp"),
            P("sp", "tp"),
            P("sp", "tp"),
            P("tp", "sp"),
            P("tp", "sp"),
            P(("sp", "tp"), None),
            P("tp", None),
            P("tp", None),
            P(),
            P("sp", "tp"),
            P("tp", "sp"),
        ),
        out_specs=P(("sp", "tp"), None),
        check_vma=False,
    )
```

profile of v0, /device:TPU:102, one launch (start us, length us, event | category | flops | bytes accessed | tf_op | source)
XLA Modules:
  0.0 342.0 jit_solution(4118133415750312991)
XLA Ops:
  8.2 1.8 concatenate.7
  10.1 1.9 fusion.43
  13.5 52.2 %all-gather.7.cloned.1.call-done = bf16[4096,515]{1,0:T(8,128)(2,1)} async-done(((bf16[256,515]{1,0:T(8,128)(2,1)}), bf16[4096,515]{1,0:T(8,128)(2,1)}) %all-gather.7.cloned.1.call-update) | async-done | bytes 4218896 | tf_op jit(solution)/shard_map/all_gather | solution.py:15
  65.7 1.3 slice_bitcast_fusion.3
  67.3 2.0 slice_reduce_fusion
  69.3 3.9 %fusion.42 = (bf16[4096,128]{1,0:T(8,128)(2,1)S(1)}, bf16[4096,128]{1,0:T(8,128)(2,1)}, bf16[4096,128]{1,0:T(8,128)(2,1)}, bf16[4096,128]{1,0:T(8,128)(2,1)}) fusion(bf16[4096,515]{1,0:T(8,128)(2,1)} %all-gather.7.cloned.1.call-done), kind=kLoop, calls=%fused_computation.76 | loop fusion | bytes 8388608 | tf_op jit(solution)/shard_map/split | solution.py:16
  73.3 191.5 %while.19 = (s32[]{:T(128)}, f32[2,256]{1,0:T(2,128)S(1)}, f32[256,2,64]{0,2,1:T(8,128)S(1)}, f32[1,256]{1,0:T(1,128)S(1)}, f32[256,1,128]{0,2,1:T(8,128)S(1)}, ...) while((s32[]{:T(128)}, f32[2,256]{1,0:T(2,128)S(1)}, ...), condition=%wide.region_7.8_spmd.clone, body=%wide.region_0.7_spmd.clone.sunk | while | flops 98831880 | bytes 9842459 | solution.py:149
  75.1 4.6 %fusion.92 = f32[2,256,2,128]{1,2,3,0:T(2,128)S(1)} fusion(f32[2,256,2,128]{1,3,2,0:T(8,128)S(1)} %bitcast.125), kind=kOutput, calls=%fused_computation.24.clone.1 | output fusion | flops 16646144 | bytes 1048576 | tf_op jit(solution)/shard_map/reduce-window.8
  81.1 1.2 fusion.96
  82.3 2.3 fusion.97
  87.0 4.6 %fusion.92 = f32[2,256,2,128]{1,2,3,0:T(2,128)S(1)} fusion(f32[2,256,2,128]{1,3,2,0:T(8,128)S(1)} %bitcast.125), kind=kOutput, calls=%fused_computation.24.clone.1 | output fusion | flops 16646144 | bytes 1048576 | tf_op jit(solution)/shard_map/reduce-window.8
  93.1 1.2 fusion.96
  94.3 2.3 fusion.97
  99.0 4.6 %fusion.92 = f32[2,256,2,128]{1,2,3,0:T(2,128)S(1)} fusion(f32[2,256,2,128]{1,3,2,0:T(8,128)S(1)} %bitcast.125), kind=kOutput, calls=%fused_computation.24.clone.1 | output fusion | flops 16646144 | bytes 1048576 | tf_op jit(solution)/shard_map/reduce-window.8
  105.0 1.2 fusion.96
  106.2 2.3 fusion.97
  111.0 4.6 %fusion.92 = f32[2,256,2,128]{1,2,3,0:T(2,128)S(1)} fusion(f32[2,256,2,128]{1,3,2,0:T(8,128)S(1)} %bitcast.125), kind=kOutput, calls=%fused_computation.24.clone.1 | output fusion | flops 16646144 | bytes 1048576 | tf_op jit(solution)/shard_map/reduce-window.8
  117.0 1.2 fusion.96
  118.2 2.3 fusion.97
  123.0 4.6 %fusion.92 = f32[2,256,2,128]{1,2,3,0:T(2,128)S(1)} fusion(f32[2,256,2,128]{1,3,2,0:T(8,128)S(1)} %bitcast.125), kind=kOutput, calls=%fused_computation.24.clone.1 | output fusion | flops 16646144 | bytes 1048576 | tf_op jit(solution)/shard_map/reduce-window.8
  129.0 1.2 fusion.96
  130.2 2.3 fusion.97
  134.9 4.6 %fusion.92 = f32[2,256,2,128]{1,2,3,0:T(2,128)S(1)} fusion(f32[2,256,2,128]{1,3,2,0:T(8,128)S(1)} %bitcast.125), kind=kOutput, calls=%fused_computation.24.clone.1 | output fusion | flops 16646144 | bytes 1048576 | tf_op jit(solution)/shard_map/reduce-window.8
  141.0 1.2 fusion.96
  142.2 2.3 fusion.97
  146.9 4.6 %fusion.92 = f32[2,256,2,128]{1,2,3,0:T(2,128)S(1)} fusion(f32[2,256,2,128]{1,3,2,0:T(8,128)S(1)} %bitcast.125), kind=kOutput, calls=%fused_computation.24.clone.1 | output fusion | flops 16646144 | bytes 1048576 | tf_op jit(solution)/shard_map/reduce-window.8
  152.9 1.2 fusion.96
  154.1 2.3 fusion.97
  158.9 4.6 %fusion.92 = f32[2,256,2,128]{1,2,3,0:T(2,128)S(1)} fusion(f32[2,256,2,128]{1,3,2,0:T(8,128)S(1)} %bitcast.125), kind=kOutput, calls=%fused_computation.24.clone.1 | output fusion | flops 16646144 | bytes 1048576 | tf_op jit(solution)/shard_map/reduce-window.8
  164.9 1.2 fusion.96
  166.1 2.3 fusion.97
  170.9 4.6 %fusion.92 = f32[2,256,2,128]{1,2,3,0:T(2,128)S(1)} fusion(f32[2,256,2,128]{1,3,2,0:T(8,128)S(1)} %bitcast.125), kind=kOutput, calls=%fused_computation.24.clone.1 | output fusion | flops 16646144 | bytes 1048576 | tf_op jit(solution)/shard_map/reduce-window.8
  176.9 1.2 fusion.96
  178.1 2.3 fusion.97
  182.8 4.6 %fusion.92 = f32[2,256,2,128]{1,2,3,0:T(2,128)S(1)} fusion(f32[2,256,2,128]{1,3,2,0:T(8,128)S(1)} %bitcast.125), kind=kOutput, calls=%fused_computation.24.clone.1 | output fusion | flops 16646144 | bytes 1048576 | tf_op jit(solution)/shard_map/reduce-window.8
  188.8 1.2 fusion.96
  190.0 2.3 fusion.97
  194.8 4.6 %fusion.92 = f32[2,256,2,128]{1,2,3,0:T(2,128)S(1)} fusion(f32[2,256,2,128]{1,3,2,0:T(8,128)S(1)} %bitcast.125), kind=kOutput, calls=%fused_computation.24.clone.1 | output fusion | flops 16646144 | bytes 1048576 | tf_op jit(solution)/shard_map/reduce-window.8
  200.8 1.2 fusion.96
  202.0 2.3 fusion.97
  206.8 4.6 %fusion.92 = f32[2,256,2,128]{1,2,3,0:T(2,128)S(1)} fusion(f32[2,256,2,128]{1,3,2,0:T(8,128)S(1)} %bitcast.125), kind=kOutput, calls=%fused_computation.24.clone.1 | output fusion | flops 16646144 | bytes 1048576 | tf_op jit(solution)/shard_map/reduce-window.8
  212.8 1.2 fusion.96
  214.0 2.3 fusion.97
  218.7 4.6 %fusion.92 = f32[2,256,2,128]{1,2,3,0:T(2,128)S(1)} fusion(f32[2,256,2,128]{1,3,2,0:T(8,128)S(1)} %bitcast.125), kind=kOutput, calls=%fused_computation.24.clone.1 | output fusion | flops 16646144 | bytes 1048576 | tf_op jit(solution)/shard_map/reduce-window.8
  224.7 1.2 fusion.96
  225.9 2.3 fusion.97
  230.7 4.6 %fusion.92 = f32[2,256,2,128]{1,2,3,0:T(2,128)S(1)} fusion(f32[2,256,2,128]{1,3,2,0:T(8,128)S(1)} %bitcast.125), kind=kOutput, calls=%fused_computation.24.clone.1 | output fusion | flops 16646144 | bytes 1048576 | tf_op jit(solution)/shard_map/reduce-window.8
  236.7 1.2 fusion.96
  237.9 2.3 fusion.97
  242.7 4.6 %fusion.92 = f32[2,256,2,128]{1,2,3,0:T(2,128)S(1)} fusion(f32[2,256,2,128]{1,3,2,0:T(8,128)S(1)} %bitcast.125), kind=kOutput, calls=%fused_computation.24.clone.1 | output fusion | flops 16646144 | bytes 1048576 | tf_op jit(solution)/shard_map/reduce-window.8
  248.7 1.2 fusion.96
  249.9 2.3 fusion.97
  254.6 4.6 %fusion.92 = f32[2,256,2,128]{1,2,3,0:T(2,128)S(1)} fusion(f32[2,256,2,128]{1,3,2,0:T(8,128)S(1)} %bitcast.125), kind=kOutput, calls=%fused_computation.24.clone.1 | output fusion | flops 16646144 | bytes 1048576 | tf_op jit(solution)/shard_map/reduce-window.8
  260.6 1.2 fusion.96
  261.8 2.3 fusion.97
  266.4 20.2 %all_to_all.15 = bf16[8,32,2048]{2,1,0:T(8,128)(2,1)S(1)} all-to-all(bf16[8,32,2048]{2,1,0:T(8,128)(2,1)S(1)} %bitcast.134), channel_id=1, replica_groups=mesh['sp'=16,'tp'=8] {'tp'}, dimensions={0} | all-to-all | bytes 2097152 | tf_op jit(solution)/shard_map/all_to_all | solution.py:33
  287.0 1.1 broadcast_in_dim.51
  288.1 4.4 %all-to-all-start.1 = ((bf16[8,32,2048]{2,1,0:T(8,128)(2,1)}), bf16[8,32,2048]{2,1,0:T(8,128)(2,1)}, u32[]{:S(2)}, u32[]{:S(2)}) async-start(bf16[8,32,2048]{2,1,0:T(8,128)(2,1)} %broadcast_in_dim.51), calls=%async_computation.1 | async-start | bytes 2097152 | tf_op jit(solution)/shard_map/all_to_all | solution.py:39
  292.6 3.5 %copy.37 = bf16[16,1024,64]{1,2,0:T(8,128)(2,1)S(1)} copy(bf16[16,1024,64]{2,1,0:T(8,128)(2,1)} %bitcast.132) | data formatting | bytes 4194304 | tf_op jit(solution)/shard_map/all_gather | solution.py:57
  296.1 4.8 %copy.39 = bf16[16,1024,64]{1,2,0:T(8,128)(2,1)} copy(bf16[16,1024,64]{2,1,0:T(8,128)(2,1)} %bitcast.133) | data formatting | bytes 4194304 | tf_op jit(solution)/shard_map/all_gather | solution.py:57
  300.9 7.4 %all-to-all-done.1 = bf16[8,32,2048]{2,1,0:T(8,128)(2,1)} async-done(((bf16[8,32,2048]{2,1,0:T(8,128)(2,1)}), bf16[8,32,2048]{2,1,0:T(8,128)(2,1)}, u32[]{:S(2)}, u32[]{:S(2)}) %all-to-all-start.1) | async-done | bytes 1048608 | tf_op jit(solution)/shard_map/all_to_all | solution.py:39
  308.3 3.8 %fusion.39 = bf16[256,1024]{1,0:T(8,128)(2,1)S(1)} fusion(bf16[256,2048]{1,0:T(8,128)(2,1)} %bitcast.6, bf16[2048,1024]{1,0:T(8,128)(2,1)} %all-gather.9.cloned.1.call-done), kind=kOutput, calls=%fused_computation.63 | convolution fusion | flops 1074528256 | bytes 5767168 | tf_op jit(solution)/shard_map/dot_general | solution.py:164
  314.6 1.1 copy.40
  316.2 18.4 %all_to_all.16 = bf16[8,32,2048]{2,1,0:T(8,128)(2,1)S(1)} all-to-all(bf16[8,32,2048]{2,1,0:T(8,128)(2,1)S(1)} %convert_element_type.70), channel_id=1, replica_groups=mesh['sp'=16,'tp'=8] {'tp'}, dimensions={0} | all-to-all | bytes 2097152 | tf_op jit(solution)/shard_map/all_to_all | solution.py:33
  (416 shorter events, 69.2 us)
Async XLA Ops:
  6.5 258.4 %copy-start = (bf16[128,2048]{1,0:T(8,128)(2,1)S(1)}, bf16[128,2048]{1,0:T(8,128)(2,1)}, u32[]{:S(2)}) copy-start(bf16[128,2048]{1,0:T(8,128)(2,1)} %param.25) | copy-start | bytes 1572868
  6.5 6.8 %copy-start.4 = (bf16[256,128]{1,0:T(8,128)(2,1)S(1)}, bf16[256,128]{1,0:T(8,128)(2,1)}, u32[]{:S(2)}) copy-start(bf16[256,128]{1,0:T(8,128)(2,1)} %param.16) | copy-start | bytes 196612
  6.5 59.1 %all-gather.7.cloned.1.call-start = ((), (), s32[]{:S(2)}) async-start(), calls=%async_computation.3 | async-start | bytes 5570560 | tf_op jit(solution)/shard_map/all_gather | solution.py:15
  10.0 282.5 %all-gather.11.cloned.1.call-start = ((), (), s32[]{:S(2)}) async-start(), calls=%async_computation.5 | async-start | bytes 4456448 | tf_op jit(solution)/shard_map/all_gather | solution.py:57
  12.0 284.1 %all-gather.13.cloned.1.call-start = ((), (), s32[]{:S(2)}) async-start(), calls=%async_computation.6 | async-start | bytes 4456448 | tf_op jit(solution)/shard_map/all_gather | solution.py:57
  12.8 288.2 %all-gather.9.cloned.1.call-start = ((), (), s32[]{:S(2)}) async-start(), calls=%async_computation.4 | async-start | bytes 4456448 | tf_op jit(solution)/shard_map/all_gather | solution.py:166
  69.3 4.0 %copy-start.6 = (bf16[256,128]{1,0:T(8,128)(2,1)S(1)}, bf16[256,128]{1,0:T(8,128)(2,1)}, u32[]{:S(2)}) copy-start(bf16[256,128]{1,0:T(8,128)(2,1)} %param.19) | copy-start | bytes 196612
  264.9 1.0 copy-start.3
  266.4 20.4 %copy-start.2 = (bf16[32,2048]{1,0:T(8,128)(2,1)S(1)}, bf16[32,2048]{1,0:T(8,128)(2,1)}, u32[]{:S(2)}) copy-start(bf16[32,2048]{1,0:T(8,128)(2,1)} %param.24) | copy-start | bytes 393220
  266.4 20.5 %copy-start.5 = (f32[2048]{0:T(1024)S(1)}, f32[2048]{0:T(1024)}, u32[]{:S(2)}) copy-start(f32[2048]{0:T(1024)} %param.27) | copy-start | bytes 24580
  288.1 20.2 %all-to-all-start.1 = ((bf16[8,32,2048]{2,1,0:T(8,128)(2,1)}), bf16[8,32,2048]{2,1,0:T(8,128)(2,1)}, u32[]{:S(2)}, u32[]{:S(2)}) async-start(bf16[8,32,2048]{2,1,0:T(8,128)(2,1)} %broadcast_in_dim.51), calls=%async_computation.1 | async-start | bytes 2097152 | tf_op jit(solution)/shard_map/all_to_all | solution.py:39
  312.1 1.6 copy-start.1
Sparse Core Ops, SparseCore 0:
  10.2 55.4 all-gather.6
  67.8 51.0 all-gather.10
  121.1 51.0 all-gather.12
  174.2 51.0 all-gather.8
where the time goes:
time: 344 us; the launch traced here: 342 us
  other arithmetic  137 us (40%)
  waiting for transfers between devices  60.9 us (18%)
  local copies, waits for them, and re-layouts  44.4 us (13%)
  matrix products  40.3 us (12%)
  blocking collectives  38.6 us (11%)
  between operations  13.4 us (4%)
  starting transfers between devices  4.56 us (1%)
    another operation x64, other arithmetic  111 us
    all_gather x1, waiting for transfers between devices, turned_gather(): whole = lax.all_gather(both, axis, axis=0, tiled=True)  52.2 us
    all_to_all x2, blocking collectives, summed_on_arrival(): tiles = lax.all_to_all(cut_along(value, dim, count), axis, 0, 0, tiled=True)  38.6 us
    dot_general x32, matrix products, stick_block(): jnp.einsum('qhe,khe->hqk', q_heads, k_heads, preferred_element_type=jnp.f...  28 us
    convert_element_type x32, other arithmetic, stick_block(): weight = weight.astype(jnp.bfloat16)  19.2 us
    dynamic_slice x48, local copies, waits for them, and re-layouts, sweep(): lax.dynamic_slice_in_dim(array, first_row, key_span, 0)  17.7 us
    all_gather x2, local copies, waits for them, and re-layouts, on_gathered_pieces(): tiles = [lax.all_gather(share, axis) for share in pieces]  8.29 us
    all_to_all x1, waiting for transfers between devices, from_everyone(): return lax.all_to_all(copies, axis, split_axis=0, concat_axis=0, tiled=True)  7.39 us
  transfers between devices with their start and end apart: 5, of which 2 were waited for; matrix products, arithmetic and copies ran while one was open for 61% of the time, Pallas kernels for 0%

commit v1 on v0

--- a/solution.py
+++ b/solution.py
@@ -12,7 +12,8 @@
     turned = [jnp.moveaxis(a, dim, 0) for a, dim in zip(arrays, dims)]
     widths = [t[0].size for t in turned]
     both = jnp.concatenate([t.reshape(-1, w) for t, w in zip(turned, widths)], axis=1)
-    whole = lax.all_gather(both, axis, axis=0, tiled=True)
+    sent = jnp.stack([both] * lax.axis_size(axis))
+    whole = jnp.concatenate(lax.all_to_all(sent, axis, 0, 0), axis=0)
     tiles = jnp.split(whole, [sum(widths[:k]) for k in range(1, len(widths))], axis=1)
     return tuple(
         (

time: 344 us -> 363 us (1.055)
  waiting for transfers between devices: 60.9 us -> 72.5 us
  starting transfers between devices: 4.56 us -> 11.6 us
    all_to_all x0 -> x1, waiting for transfers between devices: none -> 63.7 us  [turned_gather(): whole = jnp.concatenate(lax.all_to_all(sent, axis, 0, 0), axis=0)]
    all_gather x1 -> x0, waiting for transfers between devices: 52.2 us -> none  [turned_gather(): whole = lax.all_gather(both, axis, axis=0, tiled=True)]
    all_to_all x0 -> x1, starting transfers between devices: none -> 7.04 us  [turned_gather(): whole = jnp.concatenate(lax.all_to_all(sent, axis, 0, 0), axis=0)]
    split x2 -> x1, local copies, waits for them, and re-layouts: 5.9 us -> 1.79 us  [turned_gather(): jnp.split(whole, [sum(widths[:k]) for k in range(1, len(widths))], axis=1)]
    dynamic_slice x48 -> x16, local copies, waits for them, and re-layouts: 17.7 us -> 14.2 us  [sweep(): lax.dynamic_slice_in_dim(array, first_row, key_span, 0)]
  transfers between devices with their start and end apart: 5 -> 5, of which waited for: 2 -> 2; matrix products, arithmetic and copies ran while one was open for 61% -> 58% of each run, Pallas kernels for 0% -> 0%
where the time goes in v1:
time: 363 us; the launch traced here: 360 us
  other arithmetic  137 us (38%)
  waiting for transfers between devices  72.5 us (20%)
  local copies, waits for them, and re-layouts  43.3 us (12%)
  matrix products  40.1 us (11%)
  blocking collectives  39.6 us (11%)
  between operations  13.4 us (4%)
  starting transfers between devices  11.6 us (3%)
    another operation x64, other arithmetic  111 us
    all_to_all x1, waiting for transfers between devices, turned_gather(): whole = jnp.concatenate(lax.all_to_all(sent, axis, 0, 0), axis=0)  63.7 us
    all_to_all x2, blocking collectives, summed_on_arrival(): tiles = lax.all_to_all(cut_along(value, dim, count), axis, 0, 0, tiled=True)  39.6 us
    dot_general x32, matrix products, stick_block(): jnp.einsum('qhe,khe->hqk', q_heads, k_heads, preferred_element_type=jnp.f...  28.3 us
    convert_element_type x32, other arithmetic, stick_block(): weight = weight.astype(jnp.bfloat16)  19.2 us
    dynamic_slice x16, local copies, waits for them, and re-layouts, sweep(): lax.dynamic_slice_in_dim(array, first_row, key_span, 0)  14.2 us
    all_gather x2, local copies, waits for them, and re-layouts, on_gathered_pieces(): tiles = [lax.all_gather(share, axis) for share in pieces]  8.32 us
    all_to_all x1, waiting for transfers between devices, from_everyone(): return lax.all_to_all(copies, axis, split_axis=0, concat_axis=0, tiled=True)  7.33 us
  transfers between devices with their start and end apart: 5, of which 2 were waited for; matrix products, arithmetic and copies ran while one was open for 58% of the time, Pallas kernels for 0%

profile of v1, /device:TPU:102, one launch (start us, length us, event | category | flops | bytes accessed | tf_op | source)
XLA Modules:
  0.0 360.4 jit_solution(2832424891438423362)
XLA Ops:
  6.5 2.0 fusion.43
  11.4 2.3 stack.2
  13.7 7.0 %all-to-all-start = ((bf16[16,256,515]{1,2,0:T(8,128)(2,1)}), bf16[16,256,515]{1,2,0:T(8,128)(2,1)}, u32[]{:S(2)}, u32[]{:S(2)}) async-start(bf16[16,256,515]{1,2,0:T(8,128)(2,1)} %stack.2), calls=%async_computation | async-start | bytes 8519680 | tf_op jit(solution)/shard_map/all_to_all | solution.py:16
  22.3 63.7 %all-to-all-done = bf16[16,256,515]{1,2,0:T(8,128)(2,1)} async-done(((bf16[16,256,515]{1,2,0:T(8,128)(2,1)}), bf16[16,256,515]{1,2,0:T(8,128)(2,1)}, u32[]{:S(2)}, u32[]{:S(2)}) %all-to-all-start) | async-done | bytes 4218912 | tf_op jit(solution)/shard_map/all_to_all | solution.py:16
  86.1 3.1 copy.88
  89.5 3.0 copy.82
  92.4 1.8 fusion.42
  94.4 187.8 %while.19 = (s32[]{:T(128)}, f32[2,256]{1,0:T(2,128)S(1)}, f32[256,2,64]{0,2,1:T(8,128)S(1)}, f32[1,256]{1,0:T(1,128)S(1)}, f32[256,1,128]{0,2,1:T(8,128)S(1)}, ...) while((s32[]{:T(128)}, f32[2,256]{1,0:T(2,128)S(1)}, ...), condition=%wide.region_7.8_spmd.clone, body=%wide.region_0.7_spmd.clone.sunk | while | flops 98831880 | bytes 9580315 | solution.py:150
  96.2 4.6 %fusion.92 = f32[2,256,2,128]{1,2,3,0:T(2,128)S(1)} fusion(f32[2,256,2,128]{1,3,2,0:T(8,128)S(1)} %bitcast.139), kind=kOutput, calls=%fused_computation.24.clone.1 | output fusion | flops 16646144 | bytes 1048576 | tf_op jit(solution)/shard_map/reduce-window.8
  102.1 1.2 fusion.96
  103.3 2.3 fusion.97
  107.9 4.6 %fusion.92 = f32[2,256,2,128]{1,2,3,0:T(2,128)S(1)} fusion(f32[2,256,2,128]{1,3,2,0:T(8,128)S(1)} %bitcast.139), kind=kOutput, calls=%fused_computation.24.clone.1 | output fusion | flops 16646144 | bytes 1048576 | tf_op jit(solution)/shard_map/reduce-window.8
  113.8 1.2 fusion.96
  115.0 2.3 fusion.97
  119.6 4.6 %fusion.92 = f32[2,256,2,128]{1,2,3,0:T(2,128)S(1)} fusion(f32[2,256,2,128]{1,3,2,0:T(8,128)S(1)} %bitcast.139), kind=kOutput, calls=%fused_computation.24.clone.1 | output fusion | flops 16646144 | bytes 1048576 | tf_op jit(solution)/shard_map/reduce-window.8
  125.5 1.2 fusion.96
  126.7 2.3 fusion.97
  131.3 4.6 %fusion.92 = f32[2,256,2,128]{1,2,3,0:T(2,128)S(1)} fusion(f32[2,256,2,128]{1,3,2,0:T(8,128)S(1)} %bitcast.139), kind=kOutput, calls=%fused_computation.24.clone.1 | output fusion | flops 16646144 | bytes 1048576 | tf_op jit(solution)/shard_map/reduce-window.8
  137.2 1.2 fusion.96
  138.5 2.3 fusion.97
  143.1 4.6 %fusion.92 = f32[2,256,2,128]{1,2,3,0:T(2,128)S(1)} fusion(f32[2,256,2,128]{1,3,2,0:T(8,128)S(1)} %bitcast.139), kind=kOutput, calls=%fused_computation.24.clone.1 | output fusion | flops 16646144 | bytes 1048576 | tf_op jit(solution)/shard_map/reduce-window.8
  149.0 1.2 fusion.96
  150.2 2.3 fusion.97
  154.8 4.6 %fusion.92 = f32[2,256,2,128]{1,2,3,0:T(2,128)S(1)} fusion(f32[2,256,2,128]{1,3,2,0:T(8,128)S(1)} %bitcast.139), kind=kOutput, calls=%fused_computation.24.clone.1 | output fusion | flops 16646144 | bytes 1048576 | tf_op jit(solution)/shard_map/reduce-window.8
  160.7 1.2 fusion.96
  161.9 2.3 fusion.97
  166.5 4.6 %fusion.92 = f32[2,256,2,128]{1,2,3,0:T(2,128)S(1)} fusion(f32[2,256,2,128]{1,3,2,0:T(8,128)S(1)} %bitcast.139), kind=kOutput, calls=%fused_computation.24.clone.1 | output fusion | flops 16646144 | bytes 1048576 | tf_op jit(solution)/shard_map/reduce-window.8
  172.4 1.2 fusion.96
  173.7 2.3 fusion.97
  178.3 4.6 %fusion.92 = f32[2,256,2,128]{1,2,3,0:T(2,128)S(1)} fusion(f32[2,256,2,128]{1,3,2,0:T(8,128)S(1)} %bitcast.139), kind=kOutput, calls=%fused_computation.24.clone.1 | output fusion | flops 16646144 | bytes 1048576 | tf_op jit(solution)/shard_map/reduce-window.8
  184.2 1.2 fusion.96
  185.4 2.3 fusion.97
  190.0 4.6 %fusion.92 = f32[2,256,2,128]{1,2,3,0:T(2,128)S(1)} fusion(f32[2,256,2,128]{1,3,2,0:T(8,128)S(1)} %bitcast.139), kind=kOutput, calls=%fused_computation.24.clone.1 | output fusion | flops 16646144 | bytes 1048576 | tf_op jit(solution)/shard_map/reduce-window.8
  195.9 1.2 fusion.96
  197.1 2.3 fusion.97
  201.7 4.6 %fusion.92 = f32[2,256,2,128]{1,2,3,0:T(2,128)S(1)} fusion(f32[2,256,2,128]{1,3,2,0:T(8,128)S(1)} %bitcast.139), kind=kOutput, calls=%fused_computation.24.clone.1 | output fusion | flops 16646144 | bytes 1048576 | tf_op jit(solution)/shard_map/reduce-window.8
  207.6 1.2 fusion.96
  208.8 2.3 fusion.97
  213.5 4.6 %fusion.92 = f32[2,256,2,128]{1,2,3,0:T(2,128)S(1)} fusion(f32[2,256,2,128]{1,3,2,0:T(8,128)S(1)} %bitcast.139), kind=kOutput, calls=%fused_computation.24.clone.1 | output fusion | flops 16646144 | bytes 1048576 | tf_op jit(solution)/shard_map/reduce-window.8
  219.4 1.2 fusion.96
  220.6 2.3 fusion.97
  225.2 4.6 %fusion.92 = f32[2,256,2,128]{1,2,3,0:T(2,128)S(1)} fusion(f32[2,256,2,128]{1,3,2,0:T(8,128)S(1)} %bitcast.139), kind=kOutput, calls=%fused_computation.24.clone.1 | output fusion | flops 16646144 | bytes 1048576 | tf_op jit(solution)/shard_map/reduce-window.8
  231.1 1.2 fusion.96
  232.3 2.3 fusion.97
  236.9 4.6 %fusion.92 = f32[2,256,2,128]{1,2,3,0:T(2,128)S(1)} fusion(f32[2,256,2,128]{1,3,2,0:T(8,128)S(1)} %bitcast.139), kind=kOutput, calls=%fused_computation.24.clone.1 | output fusion | flops 16646144 | bytes 1048576 | tf_op jit(solution)/shard_map/reduce-window.8
  242.8 1.2 fusion.96
  244.0 2.3 fusion.97
  248.6 4.6 %fusion.92 = f32[2,256,2,128]{1,2,3,0:T(2,128)S(1)} fusion(f32[2,256,2,128]{1,3,2,0:T(8,128)S(1)} %bitcast.139), kind=kOutput, calls=%fused_computation.24.clone.1 | output fusion | flops 16646144 | bytes 1048576 | tf_op jit(solution)/shard_map/reduce-window.8
  254.5 1.2 fusion.96
  255.8 2.3 fusion.97
  260.4 4.6 %fusion.92 = f32[2,256,2,128]{1,2,3,0:T(2,128)S(1)} fusion(f32[2,256,2,128]{1,3,2,0:T(8,128)S(1)} %bitcast.139), kind=kOutput, calls=%fused_computation.24.clone.1 | output fusion | flops 16646144 | bytes 1048576 | tf_op jit(solution)/shard_map/reduce-window.8
  266.3 1.2 fusion.96
  267.5 2.3 fusion.97
  272.1 4.6 %fusion.92 = f32[2,256,2,128]{1,2,3,0:T(2,128)S(1)} fusion(f32[2,256,2,128]{1,3,2,0:T(8,128)S(1)} %bitcast.139), kind=kOutput, calls=%fused_computation.24.clone.1 | output fusion | flops 16646144 | bytes 1048576 | tf_op jit(solution)/shard_map/reduce-window.8
  278.0 1.2 fusion.96
  279.2 2.3 fusion.97
  283.7 21.2 %all_to_all.20 = bf16[8,32,2048]{2,1,0:T(8,128)(2,1)S(1)} all-to-all(bf16[8,32,2048]{2,1,0:T(8,128)(2,1)S(1)} %bitcast.148), channel_id=1, replica_groups=mesh['sp'=16,'tp'=8] {'tp'}, dimensions={0} | all-to-all | bytes 2097152 | tf_op jit(solution)/shard_map/all_to_all | solution.py:34
  305.4 1.1 broadcast_in_dim.51
  306.5 4.5 %all-to-all-start.2 = ((bf16[8,32,2048]{2,1,0:T(8,128)(2,1)}), bf16[8,32,2048]{2,1,0:T(8,128)(2,1)}, u32[]{:S(2)}, u32[]{:S(2)}) async-start(bf16[8,32,2048]{2,1,0:T(8,128)(2,1)} %broadcast_in_dim.51), calls=%async_computation.2 | async-start | bytes 2097152 | tf_op jit(solution)/shard_map/all_to_all | solution.py:40
  311.0 3.5 copy.71
  314.6 4.8 %copy.73 = bf16[16,1024,64]{1,2,0:T(8,128)(2,1)} copy(bf16[16,1024,64]{2,1,0:T(8,128)(2,1)} %bitcast.147) | data formatting | bytes 4194304 | tf_op jit(solution)/shard_map/all_gather | solution.py:58
  319.3 7.3 %all-to-all-done.2 = bf16[8,32,2048]{2,1,0:T(8,128)(2,1)} async-done(((bf16[8,32,2048]{2,1,0:T(8,128)(2,1)}), bf16[8,32,2048]{2,1,0:T(8,128)(2,1)}, u32[]{:S(2)}, u32[]{:S(2)}) %all-to-all-start.2) | async-done | bytes 1048608 | tf_op jit(solution)/shard_map/all_to_all | solution.py:40
  326.7 3.8 %fusion.39 = bf16[256,1024]{1,0:T(8,128)(2,1)S(1)} fusion(bf16[256,2048]{1,0:T(8,128)(2,1)} %bitcast.7, bf16[2048,1024]{1,0:T(8,128)(2,1)} %all-gather.6.cloned.1.call-done), kind=kOutput, calls=%fused_computation.64 | convolution fusion | flops 1074528256 | bytes 5767168 | tf_op jit(solution)/shard_map/dot_general | solution.py:165
  334.6 18.4 %all_to_all.21 = bf16[8,32,2048]{2,1,0:T(8,128)(2,1)S(1)} all-to-all(bf16[8,32,2048]{2,1,0:T(8,128)(2,1)S(1)} %convert_element_type.70), channel_id=1, replica_groups=mesh['sp'=16,'tp'=8] {'tp'}, dimensions={0} | all-to-all | bytes 2097152 | tf_op jit(solution)/shard_map/all_to_all | solution.py:34
  (386 shorter events, 67.5 us)
Async XLA Ops:
  6.5 275.7 %copy-start = (bf16[128,2048]{1,0:T(8,128)(2,1)S(1)}, bf16[128,2048]{1,0:T(8,128)(2,1)}, u32[]{:S(2)}) copy-start(bf16[128,2048]{1,0:T(8,128)(2,1)} %param.25) | copy-start | bytes 1572868
  6.5 304.4 %all-gather.8.cloned.1.call-start = ((), (), s32[]{:S(2)}) async-start(), calls=%async_computation.5 | async-start | bytes 4456448 | tf_op jit(solution)/shard_map/all_gather | solution.py:58
  13.7 8.5 %copy-start.4 = (bf16[256,128]{1,0:T(8,128)(2,1)S(1)}, bf16[256,128]{1,0:T(8,128)(2,1)}, u32[]{:S(2)}) copy-start(bf16[256,128]{1,0:T(8,128)(2,1)} %param.16) | copy-start | bytes 196612
  13.7 72.4 %all-to-all-start = ((bf16[16,256,515]{1,2,0:T(8,128)(2,1)}), bf16[16,256,515]{1,2,0:T(8,128)(2,1)}, u32[]{:S(2)}, u32[]{:S(2)}) async-start(bf16[16,256,515]{1,2,0:T(8,128)(2,1)} %stack.2), calls=%async_computation | async-start | bytes 8519680 | tf_op jit(solution)/shard_map/all_to_all | solution.py:16
  20.7 293.9 %all-gather.10.cloned.1.call-start = ((), (), s32[]{:S(2)}) async-start(), calls=%async_computation.6 | async-start | bytes 4456448 | tf_op jit(solution)/shard_map/all_gather | solution.py:58
  21.4 305.2 %all-gather.6.cloned.1.call-start = ((), (), s32[]{:S(2)}) async-start(), calls=%async_computation.4 | async-start | bytes 4456448 | tf_op jit(solution)/shard_map/all_gather | solution.py:167
  92.4 1.9 copy-start.6
  282.2 1.0 copy-start.3
  283.7 21.4 %copy-start.2 = (bf16[32,2048]{1,0:T(8,128)(2,1)S(1)}, bf16[32,2048]{1,0:T(8,128)(2,1)}, u32[]{:S(2)}) copy-start(bf16[32,2048]{1,0:T(8,128)(2,1)} %param.24) | copy-start | bytes 393220
  283.7 21.5 %copy-start.5 = (f32[2048]{0:T(1024)S(1)}, f32[2048]{0:T(1024)}, u32[]{:S(2)}) copy-start(f32[2048]{0:T(1024)} %param.27) | copy-start | bytes 24580
  306.5 20.2 %all-to-all-start.2 = ((bf16[8,32,2048]{2,1,0:T(8,128)(2,1)}), bf16[8,32,2048]{2,1,0:T(8,128)(2,1)}, u32[]{:S(2)}, u32[]{:S(2)}) async-start(bf16[8,32,2048]{2,1,0:T(8,128)(2,1)} %broadcast_in_dim.51), calls=%async_computation.2 | async-start | bytes 2097152 | tf_op jit(solution)/shard_map/all_to_all | solution.py:40
  330.5 1.6 copy-start.1
Sparse Core Ops, SparseCore 0:
  9.5 92.9 all-gather.7
  104.6 50.9 all-gather.9
  157.8 51.1 all-gather.5
